TPU v7x, 128 devices: a whole 4x4x4 slice. The times are simulated.
128 devices in a mesh: ep: 64 (over z, y, x), tp: 2 (over core).
Axes of the slice: x: 4, y: 4, z: 4, core: 2. Of those that a mesh axis runs over, the one named last changes fastest.
Arguments:
- stream: bfloat16 [4096, 2048], P('ep', 'tp'), may hold values from -40 to 40
- conv_state: bfloat16 [4096, 3, 2048], P('ep', None, 'tp'), may hold values from -5 to 5
- recur_state: float32 [4096, 2048], P('ep', 'tp'), may hold values from -5 to 5
- mix_gain: float32 [2048], replicated, may hold values from 0.1 to 1.9
- branch_weight: bfloat16 [2048, 2048], P(None, 'tp'), may hold values from -0.125 to 0.125
- gate_weight: bfloat16 [2048, 2048], P(None, 'tp'), may hold values from -0.125 to 0.125
- conv_taps: float32 [4, 2048], P(None, 'tp'), may hold values from -3 to 3
- recur_map: bfloat16 [16, 128, 128], P('tp'), may hold values from -0.5 to 0.5
- input_map: bfloat16 [16, 128, 128], P('tp'), may hold values from -0.5 to 0.5
- decay_logit: float32 [2048], P('tp'), may hold values from -1 to 6
- out_weight: bfloat16 [2048, 2048], P(None, 'tp'), may hold values from -0.125 to 0.125
- moe_gain: float32 [2048], replicated, may hold values from 0.1 to 1.9
- route_ids: int32 [4096, 6], P('ep'), may hold values from 0 to 63, all different within a row; in each aligned block of 64 rows (0 to 63, 64 to 127, ...) at most 18 rows name the same one
- route_weights: float32 [4096, 6], P('ep'), may hold values from 0.2 to 1
- expert_gate: bfloat16 [64, 2048, 512], P('ep', None, 'tp'), may hold values from -0.125 to 0.125
- expert_up: bfloat16 [64, 2048, 512], P('ep', None, 'tp'), may hold values from -0.125 to 0.125
- expert_down: bfloat16 [64, 512, 2048], P('ep', None, 'tp'), may hold values from -0.25 to 0.25
- dense_gate: bfloat16 [2048, 512], P(None, 'tp'), may hold values from -0.125 to 0.125
- dense_up: bfloat16 [2048, 512], P(None, 'tp'), may hold values from -0.125 to 0.125
- dense_down: bfloat16 [512, 2048], P(None, 'tp'), may hold values from -0.25 to 0.25
- dense_scale: float32 [2048], P('tp'), may hold values from 0.1 to 1.9
Outputs:
- result: bfloat16 [4096, 2048], P('ep', 'tp')
- new_state: float32 [4096, 2048], P('ep', 'tp')
- new_conv: bfloat16 [4096, 3, 2048], P('ep', None, 'tp')
Inputs may be any that keep to these rules, and one draw needn't show every extreme that they name: `route_ids`: each row names 6 different experts; among the rows of one index of ep no expert is named by more than 18 rows, and in every draw some expert is named by exactly 18 rows of some index.
All inputs are finite; a program needn't handle non-finite values.
Results may differ from a plain program's by a relative error of at most 0.014.
Values may be sent and summed in bfloat16 or wider, within the bound.
No kernel may reach another device: no remote copies, remote signals or barrier semaphores. Data moves between devices by JAX's collectives and lax.ppermute only.
A program may use at most 128 MiB of HBM per device.

v0:
```python
import jax
import jax.numpy as jnp
from jax import lax
from jax.sharding import PartitionSpec as P


def laid_out(tiles, dim):
    shape = list(tiles.shape[1:])
    shape[dim] *= tiles.shape[0]
    return jnp.moveaxis(tiles, 0, dim).reshape(shape)


def sent_to_all(shard, axis):
    length = lax.axis_size(axis)
    return lax.all_to_all(
        jnp.broadcast_to(shard[None], (length, *shard.shape)), axis, 0, 0, tiled=True
    )


def gathered_copies(shard, axis, dim):
    return laid_out(sent_to_all(shard, axis), dim)


def accumulate_with(weight, segment):
    return jnp.dot(segment, weight, preferred_element_type=jnp.float32)


def normalize(part_rows, gain_vec):
    whole_rows = gathered_copies(part_rows, "tp", 1).astype(jnp.float32)
    row_mean = jnp.mean(whole_rows, axis=1, keepdims=True)
    row_var = jnp.mean(whole_rows * whole_rows, axis=1, keepdims=True) - row_mean * row_mean
    return ((whole_rows - row_mean) * lax.rsqrt(row_var + 1e-05) * gain_vec).astype(jnp.bfloat16)


def per_device(
    stream,
    conv_state,
    recur_state,
    mix_gain,
    branch_weight,
    gate_weight,
    conv_taps,
    recur_map,
    input_map,
    decay_logit,
    out_weight,
    moe_gain,
    route_ids,
    route_weights,
    expert_gate,
    expert_up,
    expert_down,
    dense_gate,
    dense_up,
    dense_down,
    dense_scale,
):
    seq_count = stream.shape[0]
    out_width = stream.shape[1]
    normed = normalize(stream, mix_gain)
    branch_in = jnp.dot(normed, branch_weight, preferred_element_type=jnp.float32).astype(
        jnp.bfloat16
    )
    gate_pre = jnp.dot(normed, gate_weight, preferred_element_type=jnp.float32).astype(jnp.bfloat16)
    conv_sum = branch_in.astype(jnp.float32) * conv_taps[3]
    for offset in range(3):
        conv_sum = conv_sum + conv_state[:, offset].astype(jnp.float32) * conv_taps[offset]
    conv_out = conv_sum.astype(jnp.bfloat16)
    new_conv = jnp.concatenate([conv_state[:, 1:], branch_in[:, None]], axis=1)
    block_count = recur_map.shape[0]
    block_width = recur_map.shape[1]
    grouped = conv_out.reshape(seq_count, block_count, block_width)
    recur_gate = jax.nn.sigmoid(
        jnp.einsum("nbc,bcd->nbd", grouped, recur_map, preferred_element_type=jnp.float32)
    ).reshape(seq_count, -1)
    input_gate = jax.nn.sigmoid(
        jnp.einsum("nbc,bcd->nbd", grouped, input_map, preferred_element_type=jnp.float32)
    ).reshape(seq_count, -1)
    log_decay = -8.0 * recur_gate * jax.nn.softplus(-decay_logit)
    driven = jnp.sqrt(-jnp.expm1(2.0 * log_decay)) * (input_gate * conv_out.astype(jnp.float32))
    new_state = jnp.exp(log_decay) * recur_state + driven
    mixer_in = (jax.nn.gelu(gate_pre.astype(jnp.float32)) * new_state).astype(jnp.bfloat16)
    mixer_out = accumulate_with(
        out_weight, lax.all_gather(mixer_in, "tp", axis=1, tiled=True)
    ).astype(jnp.bfloat16)
    resid = (stream.astype(jnp.float32) + mixer_out.astype(jnp.float32)).astype(jnp.bfloat16)
    normed_two = normalize(resid, moe_gain)
    top_count = route_ids.shape[1]
    expert_count = lax.axis_size("ep")
    capacity = max(2, min(seq_count, 3 * seq_count * top_count // expert_count))
    flat_ids = route_ids.reshape(-1)
    one_hot = (flat_ids[:, None] == jnp.arange(expert_count, dtype=jnp.int32)[None, :]).astype(
        jnp.int32
    )
    slot_rank = jnp.sum(one_hot * (jnp.cumsum(one_hot, axis=0) - 1), axis=1)
    slot_index = (flat_ids * capacity + slot_rank).reshape(seq_count, top_count)
    dispatch_table = jnp.sum(
        (
            slot_index[:, :, None]
            == jnp.arange(expert_count * capacity, dtype=jnp.int32)[None, None, :]
        ).astype(jnp.bfloat16),
        axis=1,
    )
    own_gate = expert_gate[0]
    own_up = expert_up[0]
    own_down = expert_down[0]
    own_features = lax.dynamic_slice_in_dim(
        normed_two, lax.axis_index("tp") * out_width, out_width, 1
    )
    outgoing = lax.dot_general(
        dispatch_table, own_features, (((0,), (0,)), ((), ())), preferred_element_type=jnp.float32
    )
    outgoing = outgoing.astype(jnp.bfloat16).reshape(expert_count, capacity, -1)
    incoming = lax.all_gather(
        lax.all_to_all(outgoing, "ep", split_axis=0, concat_axis=0, tiled=True),
        "tp",
        axis=2,
        tiled=True,
    )
    source_count, slot_count, feature_count = incoming.shape
    taken_rows = incoming.reshape(source_count * slot_count, feature_count)
    gate_sum = jnp.dot(taken_rows, own_gate, preferred_element_type=jnp.float32)
    up_sum = jnp.dot(taken_rows, own_up, preferred_element_type=jnp.float32)
    hidden = (jax.nn.silu(gate_sum) * up_sum).astype(jnp.bfloat16)
    served_rows = accumulate_with(own_down, gathered_copies(hidden, "tp", 1))
    served = served_rows.astype(jnp.bfloat16).reshape(source_count, slot_count, -1)
    returned = lax.all_to_all(served, "ep", split_axis=0, concat_axis=0, tiled=True).reshape(
        expert_count * capacity, -1
    )
    picked = returned[slot_index]
    routed = jnp.sum(picked.astype(jnp.float32) * route_weights[:, :, None], axis=1)
    dense_gsum = jnp.dot(normed_two, dense_gate, preferred_element_type=jnp.float32)
    dense_usum = jnp.dot(normed_two, dense_up, preferred_element_type=jnp.float32)
    dense_hidden = (jax.nn.silu(dense_gsum) * dense_usum).astype(jnp.bfloat16)
    dense_out = accumulate_with(
        dense_down, lax.all_gather(dense_hidden, "tp", axis=1, tiled=True)
    ).astype(jnp.bfloat16)
    result = (
        resid.astype(jnp.float32) + routed + dense_scale * dense_out.astype(jnp.float32)
    ).astype(jnp.bfloat16)
    return (result, new_state, new_conv)


def solution(mesh):
    in_specs = (
        P("ep", "tp"),
        P("ep", None, "tp"),
        P("ep", "tp"),
        P(),
        P(None, "tp"),
        P(None, "tp"),
        P(None, "tp"),
        P("tp", None, None),
        P("tp", None, None),
        P("tp"),
        P(None, "tp"),
        P(),
        P("ep", None),
        P("ep", None),
        P("ep", None, "tp"),
        P("ep", None, "tp"),
        P("ep", None, "tp"),
        P(None, "tp"),
        P(None, "tp"),
        P(None, "tp"),
        P("tp"),
    )
    out_specs = (P("ep", "tp"), P("ep", "tp"), P("ep", None, "tp"))
    return jax.shard_map(
        per_device, mesh=mesh, in_specs=in_specs, out_specs=out_specs, check_vma=False
    )
```

profile of v0, /device:TPU:0, one launch (start us, length us, event | category | flops | bytes accessed | tf_op | source)
XLA Modules:
  0.0 197.2 jit_solution(7304002262852420736)
XLA Ops:
  7.2 0.0 copy-start
  7.2 0.0 copy-start.6
  7.2 1.7 broadcast_in_dim.10
  8.9 3.4 %all-to-all-start = ((bf16[2,64,1024]{2,1,0:T(8,128)(2,1)}), bf16[2,64,1024]{2,1,0:T(8,128)(2,1)S(1)}, u32[]{:S(2)}, u32[]{:S(2)}) async-start(bf16[2,64,1024]{2,1,0:T(8,128)(2,1)} %broadcast_in_dim.10), calls=%async_computation | async-start | bytes 524288 | tf_op jit(solution)/shard_map/all_to_all | solution.py:15
  12.4 0.9 fusion.51
  13.3 0.7 all-to-all-done
  14.0 0.2 convert_reduce_fusion.1
  14.2 0.0 copy-start.22
  14.2 0.0 copy-start.23
  14.3 4.0 %fusion.38 = (bf16[64,1024]{1,0:T(8,128)(2,1)S(1)}, bf16[64,1024]{1,0:T(8,128)(2,1)}) fusion(f32[1024]{0:T(1024)S(1)} %bitcast.101, bf16[64,3,1024]{2,0,1:T(8,128)(2,1)S(1)} %copy-done.6, f32[1024]{0:T(1024)S(1)} %bitcast.102, f32[1024]{0:T(1024)S(1)} %bitcast.100, f32[1024]{0:T(1024)S(1)} %bitcast.99, bf16[2048,1024]{1,0:T(8,128)(2,1)} %param.25, ...), kind=kOutput, calls=%fused_computation.64 | convolution fusion | flops 269811712 | bytes 5399040 | tf_op jit(solution)/shard_map/dot_general | solution.py:61
  18.2 0.2 fusion.5
  18.5 0.2 fusion.9
  18.7 0.2 copy-done.19
  18.9 0.3 copy-done.13
  19.2 0.2 fusion.36
  19.4 0.0 copy-start.9
  19.5 1.0 fusion.34
  20.5 2.1 %all_gather.9 = bf16[64,2048]{1,0:T(8,128)(2,1)S(1)} all-gather(bf16[64,1024]{1,0:T(8,128)(2,1)S(1)} %fusion.34), channel_id=1, replica_groups=mesh['ep'=64,'tp'=2] {'tp'}, dimensions={1}, use_global_device_ids=true | all-gather | bytes 393216 | tf_op jit(solution)/shard_map/all_gather | solution.py:84
  22.6 0.9 fusion.15
  23.5 0.7 broadcast_in_dim.11
  24.2 3.4 %all-to-all-start.1 = ((bf16[2,64,1024]{2,1,0:T(8,128)(2,1)}), bf16[2,64,1024]{2,1,0:T(8,128)(2,1)S(1)}, u32[]{:S(2)}, u32[]{:S(2)}) async-start(bf16[2,64,1024]{2,1,0:T(8,128)(2,1)} %broadcast_in_dim.11), calls=%async_computation.1 | async-start | bytes 524288 | tf_op jit(solution)/shard_map/all_to_all | solution.py:15
  27.6 0.0 all-gather.2.cloned.1.call-start
  27.7 0.1 copy.73
  27.8 0.1 eq.38
  27.9 0.1 eq.42
  28.1 1.1 all-to-all-done.1
  29.3 0.9 reduce-window.6
  30.2 0.2 slice_reduce_fusion
  30.5 0.1 fusion.47
  30.6 0.1 reduce_sum.71
  30.7 0.1 copy.76
  30.8 1.0 fusion.23
  31.8 0.2 convert_reduce_fusion
  32.0 0.1 multiply_convert_fusion
  32.2 0.7 copy-done.4
  32.9 1.7 convolution_convert_fusion.1
  34.6 2.4 %reshape.118 = bf16[64,18,1024]{2,1,0:T(8,128)(2,1)} reshape(bf16[1152,1024]{1,0:T(8,128)(2,1)S(1)} %convolution_convert_fusion.1) | data formatting | bytes 4718592 | tf_op jit(solution)/shard_map/reshape | solution.py:113
  37.0 53.3 %all_to_all.25 = bf16[64,18,1024]{2,1,0:T(8,128)(2,1)} all-to-all(bf16[64,18,1024]{2,1,0:T(8,128)(2,1)} %reshape.118), channel_id=1, replica_groups=mesh['ep'=64,'tp'=2] {'ep'}, dimensions={0} | all-to-all | bytes 4718592 | tf_op jit(solution)/shard_map/all_to_all | solution.py:115
  90.3 0.0 all-gather.2.cloned.1.call-update
  90.3 15.6 %all-gather.2.cloned.1.call-done = bf16[64,18,2048]{2,1,0:T(8,128)(2,1)} async-done(((bf16[64,18,1024]{2,1,0:T(8,128)(2,1)}), bf16[64,18,2048]{2,1,0:T(8,128)(2,1)}) %all-gather.2.cloned.1.call-update) | async-done | bytes 4718608 | tf_op jit(solution)/shard_map/all_gather | solution.py:114
  106.0 7.8 %reshape.119 = bf16[1152,2048]{1,0:T(8,128)(2,1)} reshape(bf16[64,18,2048]{2,1,0:T(8,128)(2,1)} %all-gather.2.cloned.1.call-done) | data formatting | bytes 9437184 | tf_op jit(solution)/shard_map/reshape | solution.py:121
  113.7 3.9 %fusion.21 = f32[1152,256]{1,0:T(8,128)S(1)} fusion(bf16[1152,2048]{1,0:T(8,128)(2,1)} %reshape.119, bf16[1,2048,256]{2,1,0:T(8,128)(2,1)S(1)} %copy-done.20), kind=kOutput, calls=%fused_computation.34 | convolution fusion | flops 1207959552 | bytes 6946816 | tf_op jit(solution)/shard_map/dot_general | solution.py:122
  117.7 0.1 copy-done.21
  117.8 1.6 fusion
  119.4 0.3 copy.78
  119.7 0.1 broadcast_in_dim.12
  119.8 4.7 %all_to_all.26 = bf16[2,1152,256]{1,2,0:T(8,128)(2,1)S(1)} all-to-all(bf16[2,1152,256]{1,2,0:T(8,128)(2,1)S(1)} %broadcast_in_dim.12), channel_id=1, replica_groups=mesh['ep'=64,'tp'=2] {'tp'}, dimensions={0} | all-to-all | bytes 2359296 | tf_op jit(solution)/shard_map/all_to_all | solution.py:15
  124.4 1.4 convolution_convert_fusion
  125.9 2.4 %reshape.121 = bf16[64,18,1024]{2,1,0:T(8,128)(2,1)} reshape(bf16[1152,1024]{1,0:T(8,128)(2,1)S(1)} %convolution_convert_fusion) | data formatting | bytes 4718592 | tf_op jit(solution)/shard_map/reshape | solution.py:126
  128.3 10.8 %all-to-all-start.4 = ((bf16[64,18,1024]{2,1,0:T(8,128)(2,1)}), bf16[64,18,1024]{2,1,0:T(8,128)(2,1)}, u32[]{:S(2)}, u32[]{:S(2)}) async-start(bf16[64,18,1024]{2,1,0:T(8,128)(2,1)} %reshape.121), calls=%async_computation.4 | async-start | bytes 6291456 | tf_op jit(solution)/shard_map/all_to_all | solution.py:127
  139.1 0.0 slice-start
  139.1 0.1 copy.79
  139.2 0.1 reshape.130
  139.3 0.7 copy.80
  140.1 0.3 fusion.52
  140.4 1.5 fusion.18
  141.9 2.0 %all_gather.11 = bf16[64,512]{1,0:T(8,128)(2,1)} all-gather(bf16[64,256]{1,0:T(8,128)(2,1)S(1)} %fusion.18), channel_id=1, replica_groups=mesh['ep'=64,'tp'=2] {'tp'}, dimensions={1}, use_global_device_ids=true | all-gather | bytes 98304 | tf_op jit(solution)/shard_map/all_gather | solution.py:136
  143.9 0.8 pad_maximum_fusion
  144.7 36.2 %all-to-all-done.4 = bf16[64,18,1024]{2,1,0:T(8,128)(2,1)} async-done(((bf16[64,18,1024]{2,1,0:T(8,128)(2,1)}), bf16[64,18,1024]{2,1,0:T(8,128)(2,1)}, u32[]{:S(2)}, u32[]{:S(2)}) %all-to-all-start.4) | async-done | bytes 2359328 | tf_op jit(solution)/shard_map/all_to_all | solution.py:127
  180.9 2.9 %reshape.122 = bf16[1152,1024]{1,0:T(8,128)(2,1)S(1)} reshape(bf16[64,18,1024]{2,1,0:T(8,128)(2,1)} %all-to-all-done.4) | data formatting | bytes 4718592 | tf_op jit(solution)/shard_map/reshape | solution.py:127
  183.8 2.7 %gather_fusion = bf16[384,1024]{1,0:T(8,128)(2,1)} fusion(bf16[1152,1024]{1,0:T(8,128)(2,1)S(1)} %reshape.122, s32[1024]{0:T(1024)S(1)} %pad_clamp_fusion), kind=kCustom, calls=%fused_computation | custom fusion | bytes 1574400 | tf_op jit(solution)/shard_map/gather | solution.py:130
  186.5 1.3 reshape.138
  187.8 1.6 multiply_reduce_fusion
  189.4 1.0 fusion.17
  (51 shorter events, 0.3 us)
Async XLA Ops:
  7.2 117.3 %copy-start = (bf16[1,512,1024]{2,1,0:T(8,128)(2,1)S(1)}, bf16[1,512,1024]{2,1,0:T(8,128)(2,1)}, u32[]{:S(2)}) copy-start(bf16[1,512,1024]{2,1,0:T(8,128)(2,1)} %param.37) | copy-start | bytes 3145732
  7.2 7.0 %copy-start.6 = (bf16[64,3,1024]{2,0,1:T(8,128)(2,1)S(1)}, bf16[64,3,1024]{2,0,1:T(8,128)(2,1)}, u32[]{:S(2)}) copy-start(bf16[64,3,1024]{2,0,1:T(8,128)(2,1)} %param.22) | copy-start | bytes 1179652
  7.2 7.0 %copy-start.14 = (f32[2048]{0:T(1024)S(1)}, f32[2048]{0:T(1024)}, u32[]{:S(2)}) copy-start(f32[2048]{0:T(1024)} %param.24) | copy-start | bytes 24580
  8.9 5.0 %all-to-all-start = ((bf16[2,64,1024]{2,1,0:T(8,128)(2,1)}), bf16[2,64,1024]{2,1,0:T(8,128)(2,1)S(1)}, u32[]{:S(2)}, u32[]{:S(2)}) async-start(bf16[2,64,1024]{2,1,0:T(8,128)(2,1)} %broadcast_in_dim.10), calls=%async_computation | async-start | bytes 524288 | tf_op jit(solution)/shard_map/all_to_all | solution.py:15
  14.2 4.0 %copy-start.22 = (bf16[8,128,128]{2,1,0:T(8,128)(2,1)S(1)}, bf16[8,128,128]{2,1,0:T(8,128)(2,1)}, u32[]{:S(2)}) copy-start(bf16[8,128,128]{2,1,0:T(8,128)(2,1)} %param.29) | copy-start | bytes 786436
  14.2 4.2 %copy-start.23 = (bf16[8,128,128]{2,1,0:T(8,128)(2,1)S(1)}, bf16[8,128,128]{2,1,0:T(8,128)(2,1)}, u32[]{:S(2)}) copy-start(bf16[8,128,128]{2,1,0:T(8,128)(2,1)} %param.28) | copy-start | bytes 786436
  14.3 5.2 %copy-start.3 = (bf16[2048,1024]{1,0:T(8,128)(2,1)S(1)}, bf16[2048,1024]{1,0:T(8,128)(2,1)}, u32[]{:S(2)}) copy-start(bf16[2048,1024]{1,0:T(8,128)(2,1)} %param.26) | copy-start | bytes 12582916
  18.2 0.7 copy-start.19
  18.2 1.0 copy-start.13
  19.4 1.0 copy-start.9
  19.4 3.1 %copy-start.2 = (bf16[2048,1024]{1,0:T(8,128)(2,1)S(1)}, bf16[2048,1024]{1,0:T(8,128)(2,1)}, u32[]{:S(2)}) copy-start(bf16[2048,1024]{1,0:T(8,128)(2,1)} %param.31) | copy-start | bytes 12582916
  19.5 3.1 %copy-start.10 = (bf16[64,1024]{1,0:T(8,128)(2,1)S(1)}, bf16[64,1024]{1,0:T(8,128)(2,1)}, u32[]{:S(2)}) copy-start(bf16[64,1024]{1,0:T(8,128)(2,1)} %param.21) | copy-start | bytes 393220
  22.6 5.1 %copy-start.15 = (s32[64,6]{0,1:T(8,128)S(1)}, s32[64,6]{0,1:T(8,128)}, u32[]{:S(2)}) copy-start(s32[64,6]{0,1:T(8,128)} %param.33) | copy-start | bytes 4612
  23.4 8.6 %copy-start.16 = (f32[2048]{0:T(1024)S(1)}, f32[2048]{0:T(1024)}, u32[]{:S(2)}) copy-start(f32[2048]{0:T(1024)} %param.32) | copy-start | bytes 24580
  24.2 5.0 %all-to-all-start.1 = ((bf16[2,64,1024]{2,1,0:T(8,128)(2,1)}), bf16[2,64,1024]{2,1,0:T(8,128)(2,1)S(1)}, u32[]{:S(2)}, u32[]{:S(2)}) async-start(bf16[2,64,1024]{2,1,0:T(8,128)(2,1)} %broadcast_in_dim.11), calls=%async_computation.1 | async-start | bytes 524288 | tf_op jit(solution)/shard_map/all_to_all | solution.py:15
  27.6 78.3 %all-gather.2.cloned.1.call-start = ((), (), s32[]{:S(2)}) async-start(), calls=%async_computation.5 | async-start | bytes 9437184 | tf_op jit(solution)/shard_map/all_gather | solution.py:114
  32.1 0.7 copy-start.4
  90.3 23.4 %copy-start.20 = (bf16[1,2048,256]{2,1,0:T(8,128)(2,1)S(1)}, bf16[1,2048,256]{2,1,0:T(8,128)(2,1)}, u32[]{:S(2)}) copy-start(bf16[1,2048,256]{2,1,0:T(8,128)(2,1)} %param.35) | copy-start | bytes 3145732
  113.7 3.9 %copy-start.1 = (bf16[1152,2048]{1,0:T(8,128)(2,1)S(1)}, bf16[1152,2048]{1,0:T(8,128)(2,1)}, u32[]{:S(2)}) copy-start(bf16[1152,2048]{1,0:T(8,128)(2,1)} %reshape.119) | copy-start | bytes 14155780
  113.7 4.1 %copy-start.21 = (bf16[1,2048,256]{2,1,0:T(8,128)(2,1)S(1)}, bf16[1,2048,256]{2,1,0:T(8,128)(2,1)}, u32[]{:S(2)}) copy-start(bf16[1,2048,256]{2,1,0:T(8,128)(2,1)} %param.36) | copy-start | bytes 3145732
  128.3 11.0 %copy-start.18 = (f32[64,6]{0,1:T(8,128)S(1)}, f32[64,6]{0,1:T(8,128)}, u32[]{:S(2)}) copy-start(f32[64,6]{0,1:T(8,128)} %param.34) | copy-start | bytes 4612
  128.3 11.7 %copy-start.5 = (bf16[64,2048]{1,0:T(8,128)(2,1)S(1)}, bf16[64,2048]{1,0:T(8,128)(2,1)}, u32[]{:S(2)}) copy-start(bf16[64,2048]{1,0:T(8,128)(2,1)} %copy-done.4) | copy-start | bytes 786436
  128.3 11.7 %copy-start.7 = (bf16[2048,256]{1,0:T(8,128)(2,1)S(1)}, bf16[2048,256]{1,0:T(8,128)(2,1)}, u32[]{:S(2)}) copy-start(bf16[2048,256]{1,0:T(8,128)(2,1)} %param.38) | copy-start | bytes 3145732
  128.3 52.5 %all-to-all-start.4 = ((bf16[64,18,1024]{2,1,0:T(8,128)(2,1)}), bf16[64,18,1024]{2,1,0:T(8,128)(2,1)}, u32[]{:S(2)}, u32[]{:S(2)}) async-start(bf16[64,18,1024]{2,1,0:T(8,128)(2,1)} %reshape.121), calls=%async_computation.4 | async-start | bytes 6291456 | tf_op jit(solution)/shard_map/all_to_all | solution.py:127
  139.1 4.8 %slice-start = ((bf16[64,3,1024]{2,0,1:T(8,128)(2,1)}), bf16[64,2,1024]{2,0,1:T(8,128)(2,1)S(1)}, s32[]{:S(2)}) async-start(bf16[64,3,1024]{2,0,1:T(8,128)(2,1)} %param.22), calls=%async_computation.6 | async-start | bytes 524288 | tf_op jit(solution)/shard_map/slice | solution.py:69
  139.1 4.8 %copy-start.11 = (bf16[64,1024]{1,0:T(8,128)(2,1)S(1)}, bf16[64,1024]{1,0:T(8,128)(2,1)}, u32[]{:S(2)}) copy-start(bf16[64,1024]{1,0:T(8,128)(2,1)} %get-tuple-element.18) | copy-start | bytes 393220
  186.5 2.9 %copy-start.17 = (f32[1024]{0:T(1024)S(1)}, f32[1024]{0:T(1024)}, u32[]{:S(2)}) copy-start(f32[1024]{0:T(1024)} %param.41) | copy-start | bytes 12292
  187.8 1.6 copy-start.8
  187.8 1.6 copy-start.12
Sparse Core Ops, SparseCore 0:
  90.4 15.4 all-gather.1
where the time goes:
time: 198 us; the launch traced here: 197 us
  blocking collectives  62.1 us (31%)
  waiting for transfers between devices  53.6 us (27%)
  local copies, waits for them, and re-layouts  26.5 us (13%)
  starting transfers between devices  17.7 us (9%)
  matrix products  17.6 us (9%)
  between operations  14.5 us (7%)
  other arithmetic  5.26 us (3%)
    all_to_all x1, blocking collectives, per_device(): lax.all_to_all(outgoing, 'ep', split_axis=0, concat_axis=0, tiled=True)  53.3 us
    all_to_all x1, waiting for transfers between devices, per_device(): lax.all_to_all(served, 'ep', split_axis=0, concat_axis=0, tiled=True)  36.2 us
    all_gather x1, waiting for transfers between devices, per_device(): lax.all_gather(lax.all_to_all(outgoing, 'ep', split_axis=0, concat_axis=0...  15.6 us
    all_to_all x1, starting transfers between devices, per_device(): lax.all_to_all(served, 'ep', split_axis=0, concat_axis=0, tiled=True)  10.8 us
    reshape x1, local copies, waits for them, and re-layouts, per_device(): taken_rows = incoming.reshape(source_count * slot_count, feature_count)  7.77 us
    all_to_all x2, starting transfers between devices, sent_to_all(): lax.all_to_all(jnp.broadcast_to(shard[None], (length, *shard.shape)), axi...  6.89 us
    all_to_all x1, blocking collectives, sent_to_all(): lax.all_to_all(jnp.broadcast_to(shard[None], (length, *shard.shape)), axi...  4.68 us
  transfers between devices with their start and end apart: 4, of which 4 were waited for; matrix products, arithmetic and copies ran while one was open for 2% of the time, Pallas kernels for 0%

commit v1 on v0

--- a/solution.py
+++ b/solution.py
@@ -111,12 +111,9 @@
         dispatch_table, own_features, (((0,), (0,)), ((), ())), preferred_element_type=jnp.float32
     )
     outgoing = outgoing.astype(jnp.bfloat16).reshape(expert_count, capacity, -1)
-    incoming = lax.all_gather(
-        lax.all_to_all(outgoing, "ep", split_axis=0, concat_axis=0, tiled=True),
-        "tp",
-        axis=2,
-        tiled=True,
-    )
+    block = lax.all_to_all(outgoing, "ep", split_axis=0, concat_axis=0, tiled=True)
+    sent = jnp.stack([block] * lax.axis_size("tp"))
+    incoming = jnp.concatenate(lax.all_to_all(sent, "tp", 0, 0), axis=2)
     source_count, slot_count, feature_count = incoming.shape
     taken_rows = incoming.reshape(source_count * slot_count, feature_count)
     gate_sum = jnp.dot(taken_rows, own_gate, preferred_element_type=jnp.float32)

time: 198 us -> 181 us (0.914)
  waiting for transfers between devices: 53.6 us -> 38.7 us
  between operations: 14.5 us -> 1.09 us
  blocking collectives: 62.1 us -> 70.6 us
  local copies, waits for them, and re-layouts: 26.5 us -> 34.4 us
  starting transfers between devices: 17.7 us -> 12.8 us
    all_gather x1 -> x0, waiting for transfers between devices: 15.6 us -> none  [per_device(): lax.all_gather(lax.all_to_all(outgoing, 'ep', split_axis=0, concat_axis=0...]
    all_to_all x0 -> x1, blocking collectives: none -> 8.61 us  [per_device(): incoming = jnp.concatenate(lax.all_to_all(sent, 'tp', 0, 0), axis=2)]
    all_to_all x1, starting transfers between devices: 10.8 us -> 5.93 us  [per_device(): lax.all_to_all(served, 'ep', split_axis=0, concat_axis=0, tiled=True)]
    unnamed x50 -> x45, local copies, waits for them, and re-layouts: 2.22 us -> 5.96 us
    another operation x0 -> x1, local copies, waits for them, and re-layouts: none -> 2.63 us  [per_device(): sent = jnp.stack([block] * lax.axis_size('tp'))]
    dot_general x1, matrix products: 3.9 us -> 1.41 us  [per_device(): gate_sum = jnp.dot(taken_rows, own_gate, preferred_element_type=jnp.float32)]
  transfers between devices with their start and end apart: 4 -> 3, of which waited for: 4 -> 3; matrix products, arithmetic and copies ran while one was open for 2% -> 3% of each run, Pallas kernels for 0% -> 0%
where the time goes in v1:
time: 181 us; the launch traced here: 180 us
  blocking collectives  70.6 us (39%)
  waiting for transfers between devices  38.7 us (21%)
  local copies, waits for them, and re-layouts  34.4 us (19%)
  matrix products  16.4 us (9%)
  starting transfers between devices  12.8 us (7%)
  other arithmetic  6.09 us (3%)
    all_to_all x1, blocking collectives, per_device(): lax.all_to_all(outgoing, 'ep', split_axis=0, concat_axis=0, tiled=True)  53.2 us
    all_to_all x1, waiting for transfers between devices, per_device(): lax.all_to_all(served, 'ep', split_axis=0, concat_axis=0, tiled=True)  36.9 us
    reshape x1, local copies, waits for them, and re-layouts, per_device(): incoming = jnp.concatenate(lax.all_to_all(sent, 'tp', 0, 0), axis=2)  9.36 us
    all_to_all x1, blocking collectives, per_device(): incoming = jnp.concatenate(lax.all_to_all(sent, 'tp', 0, 0), axis=2)  8.61 us
    all_to_all x2, starting transfers between devices, sent_to_all(): lax.all_to_all(jnp.broadcast_to(shard[None], (length, *shard.shape)), axi...  6.89 us
    unnamed x45, local copies, waits for them, and re-layouts  5.96 us
    all_to_all x1, starting transfers between devices, per_device(): lax.all_to_all(served, 'ep', split_axis=0, concat_axis=0, tiled=True)  5.93 us
    all_to_all x1, blocking collectives, sent_to_all(): lax.all_to_all(jnp.broadcast_to(shard[None], (length, *shard.shape)), axi...  4.68 us
  transfers between devices with their start and end apart: 3, of which 3 were waited for; matrix products, arithmetic and copies ran while one was open for 3% of the time, Pallas kernels for 0%

profile of v1, /device:TPU:0, one launch (start us, length us, event | category | flops | bytes accessed | tf_op | source)
XLA Modules:
  0.0 180.1 jit_solution(7945209582787277370)
XLA Ops:
  0.6 0.0 copy-start
  0.7 1.7 broadcast_in_dim.10
  2.4 3.4 %all-to-all-start = ((bf16[2,64,1024]{2,1,0:T(8,128)(2,1)}), bf16[2,64,1024]{2,1,0:T(8,128)(2,1)S(1)}, u32[]{:S(2)}, u32[]{:S(2)}) async-start(bf16[2,64,1024]{2,1,0:T(8,128)(2,1)} %broadcast_in_dim.10), calls=%async_computation | async-start | bytes 524288 | tf_op jit(solution)/shard_map/all_to_all | solution.py:15
  5.9 0.9 fusion.51
  6.7 0.7 all-to-all-done
  7.4 0.0 copy-start.19
  7.5 0.2 convert_reduce_fusion.1
  7.7 0.0 copy-start.10
  7.7 0.0 copy-start.2
  7.7 4.0 %fusion.38 = (bf16[64,1024]{1,0:T(8,128)(2,1)S(1)}, bf16[64,1024]{1,0:T(8,128)(2,1)}) fusion(f32[1024]{0:T(1024)S(1)} %bitcast.111, bf16[64,3,1024]{2,0,1:T(8,128)(2,1)S(1)} %copy-done.5, f32[1024]{0:T(1024)S(1)} %bitcast.112, f32[1024]{0:T(1024)S(1)} %bitcast.110, f32[1024]{0:T(1024)S(1)} %bitcast.109, bf16[2048,1024]{1,0:T(8,128)(2,1)} %param.25, ...), kind=kOutput, calls=%fused_computation.65 | convolution fusion | flops 269811712 | bytes 5399040 | tf_op jit(solution)/shard_map/dot_general | solution.py:61
  11.7 0.2 fusion.5
  12.0 0.2 fusion.9
  12.2 0.0 copy-start.1
  12.3 0.0 copy-start.8
  12.3 0.2 fusion.36
  12.5 1.0 fusion.34
  13.5 2.1 %all_gather.6 = bf16[64,2048]{1,0:T(8,128)(2,1)S(1)} all-gather(bf16[64,1024]{1,0:T(8,128)(2,1)S(1)} %fusion.34), channel_id=1, replica_groups=mesh['ep'=64,'tp'=2] {'tp'}, dimensions={1}, use_global_device_ids=true | all-gather | bytes 393216 | tf_op jit(solution)/shard_map/all_gather | solution.py:84
  15.6 0.9 fusion.15
  16.5 0.7 broadcast_in_dim.11
  17.3 3.4 %all-to-all-start.1 = ((bf16[2,64,1024]{2,1,0:T(8,128)(2,1)}), bf16[2,64,1024]{2,1,0:T(8,128)(2,1)S(1)}, u32[]{:S(2)}, u32[]{:S(2)}) async-start(bf16[2,64,1024]{2,1,0:T(8,128)(2,1)} %broadcast_in_dim.11), calls=%async_computation.1 | async-start | bytes 524288 | tf_op jit(solution)/shard_map/all_to_all | solution.py:15
  20.7 0.1 copy.78
  20.8 0.1 eq.38
  21.0 0.1 eq.42
  21.1 1.1 all-to-all-done.1
  22.4 0.9 reduce-window.6
  23.3 0.2 slice_reduce_fusion
  23.5 0.1 fusion.47
  23.6 0.1 reduce_sum.71
  23.8 0.1 copy.81
  23.9 1.0 fusion.23
  24.9 0.2 convert_reduce_fusion
  25.1 0.1 multiply_convert_fusion
  25.2 0.7 copy-done.3
  25.9 1.7 convolution_convert_fusion.1
  27.6 2.4 %reshape.118 = bf16[64,18,1024]{2,1,0:T(8,128)(2,1)} reshape(bf16[1152,1024]{1,0:T(8,128)(2,1)S(1)} %convolution_convert_fusion.1) | data formatting | bytes 4718592 | tf_op jit(solution)/shard_map/reshape | solution.py:113
  30.0 53.2 %all_to_all.30 = bf16[64,18,1024]{2,1,0:T(8,128)(2,1)S(1)} all-to-all(bf16[64,18,1024]{2,1,0:T(8,128)(2,1)} %reshape.118), channel_id=1, replica_groups=mesh['ep'=64,'tp'=2] {'ep'}, dimensions={0} | all-to-all | bytes 4718592 | tf_op jit(solution)/shard_map/all_to_all | solution.py:114
  83.2 0.9 pad_maximum_fusion
  84.1 2.6 %copy.83 = bf16[2,64,18,1024]{3,1,2,0:T(8,128)(2,1)S(1)} copy(bf16[2,64,18,1024]{3,2,1,0:T(8,128)(2,1)S(1)} %pad_maximum_fusion) | data formatting | bytes 9437184 | tf_op jit(solution)/shard_map/stack | solution.py:115
  86.8 8.6 %all_to_all.31 = bf16[2,64,18,1024]{3,1,2,0:T(8,128)(2,1)} all-to-all(bf16[2,64,18,1024]{3,1,2,0:T(8,128)(2,1)S(1)} %copy.83), channel_id=1, replica_groups=mesh['ep'=64,'tp'=2] {'tp'}, dimensions={0} | all-to-all | bytes 9437184 | tf_op jit(solution)/shard_map/all_to_all | solution.py:116
  95.4 9.4 %copy.84 = bf16[64,18,2,1024]{3,2,1,0:T(2,128)(2,1)} copy(bf16[64,18,2,1024]{3,0,1,2:T(8,128)(2,1)} %bitcast.99) | data formatting | bytes 9437184 | tf_op jit(solution)/shard_map/reshape | solution.py:116
  104.7 4.4 %copy.94 = bf16[144,8,2,1024]{3,1,2,0:T(8,128)(2,1)S(1)} copy(bf16[144,8,2,1024]{3,2,1,0:T(2,128)(2,1)} %bitcast.100) | data formatting | bytes 9437184
  109.1 0.0 copy-start.18
  109.1 1.4 fusion.21
  110.6 1.6 fusion
  112.1 0.3 copy.85
  112.4 0.1 broadcast_in_dim.12
  112.5 4.7 %all_to_all.32 = bf16[2,1152,256]{1,2,0:T(8,128)(2,1)S(1)} all-to-all(bf16[2,1152,256]{1,2,0:T(8,128)(2,1)S(1)} %broadcast_in_dim.12), channel_id=1, replica_groups=mesh['ep'=64,'tp'=2] {'tp'}, dimensions={0} | all-to-all | bytes 2359296 | tf_op jit(solution)/shard_map/all_to_all | solution.py:15
  117.2 1.4 convolution_convert_fusion
  118.6 2.4 %reshape.121 = bf16[64,18,1024]{2,1,0:T(8,128)(2,1)} reshape(bf16[1152,1024]{1,0:T(8,128)(2,1)S(1)} %convolution_convert_fusion) | data formatting | bytes 4718592 | tf_op jit(solution)/shard_map/reshape | solution.py:123
  121.0 5.9 %all-to-all-start.5 = ((bf16[64,18,1024]{2,1,0:T(8,128)(2,1)}), bf16[64,18,1024]{2,1,0:T(8,128)(2,1)}, u32[]{:S(2)}, u32[]{:S(2)}) async-start(bf16[64,18,1024]{2,1,0:T(8,128)(2,1)} %reshape.121), calls=%async_computation.5 | async-start | bytes 6291456 | tf_op jit(solution)/shard_map/all_to_all | solution.py:124
  127.0 0.0 slice-start
  127.0 0.1 copy.86
  127.1 0.1 reshape.130
  127.3 0.7 copy.87
  128.0 0.3 fusion.52
  128.3 1.5 fusion.18
  129.8 2.0 %all_gather.7 = bf16[64,512]{1,0:T(8,128)(2,1)} all-gather(bf16[64,256]{1,0:T(8,128)(2,1)S(1)} %fusion.18), channel_id=1, replica_groups=mesh['ep'=64,'tp'=2] {'tp'}, dimensions={1}, use_global_device_ids=true | all-gather | bytes 98304 | tf_op jit(solution)/shard_map/all_gather | solution.py:133
  131.8 0.8 pad_maximum_fusion.1
  132.6 36.9 %all-to-all-done.5 = bf16[64,18,1024]{2,1,0:T(8,128)(2,1)} async-done(((bf16[64,18,1024]{2,1,0:T(8,128)(2,1)}), bf16[64,18,1024]{2,1,0:T(8,128)(2,1)}, u32[]{:S(2)}, u32[]{:S(2)}) %all-to-all-start.5) | async-done | bytes 2359328 | tf_op jit(solution)/shard_map/all_to_all | solution.py:124
  169.4 2.9 %reshape.122 = bf16[1152,1024]{1,0:T(8,128)(2,1)S(1)} reshape(bf16[64,18,1024]{2,1,0:T(8,128)(2,1)} %all-to-all-done.5) | data formatting | bytes 4718592 | tf_op jit(solution)/shard_map/reshape | solution.py:124
  172.4 2.7 %gather_fusion = bf16[384,1024]{1,0:T(8,128)(2,1)} fusion(bf16[1152,1024]{1,0:T(8,128)(2,1)S(1)} %reshape.122, s32[1024]{0:T(1024)S(1)} %pad_clamp_fusion), kind=kCustom, calls=%fused_computation | custom fusion | bytes 1574400 | tf_op jit(solution)/shard_map/gather | solution.py:127
  175.1 1.3 reshape.138
  176.4 1.5 multiply_reduce_fusion
  177.9 2.2 %fusion.17 = bf16[64,1024]{1,0:T(8,128)(2,1)} fusion(bf16[64,512]{1,0:T(8,128)(2,1)} %all_gather.7, bf16[512,1024]{1,0:T(8,128)(2,1)} %param.40, f32[64,1024]{1,0:T(8,128)S(1)} %multiply_reduce_fusion, bf16[64,1024]{1,0:T(8,128)(2,1)S(1)} %fusion.15, f32[1024]{0:T(1024)S(1)} %copy-done.14), kind=kOutput, calls=%fused_computation.30 | convolution fusion | flops 67567616 | bytes 1642496 | tf_op jit(solution)/shard_map/dot_general | solution.py:25
  (46 shorter events, 0.3 us)
Async XLA Ops:
  0.6 116.6 %copy-start = (bf16[1,512,1024]{2,1,0:T(8,128)(2,1)S(1)}, bf16[1,512,1024]{2,1,0:T(8,128)(2,1)}, u32[]{:S(2)}) copy-start(bf16[1,512,1024]{2,1,0:T(8,128)(2,1)} %param.37) | copy-start | bytes 3145732
  0.6 7.0 %copy-start.5 = (bf16[64,3,1024]{2,0,1:T(8,128)(2,1)S(1)}, bf16[64,3,1024]{2,0,1:T(8,128)(2,1)}, u32[]{:S(2)}) copy-start(bf16[64,3,1024]{2,0,1:T(8,128)(2,1)} %param.22) | copy-start | bytes 1179652
  2.4 5.0 %all-to-all-start = ((bf16[2,64,1024]{2,1,0:T(8,128)(2,1)}), bf16[2,64,1024]{2,1,0:T(8,128)(2,1)S(1)}, u32[]{:S(2)}, u32[]{:S(2)}) async-start(bf16[2,64,1024]{2,1,0:T(8,128)(2,1)} %broadcast_in_dim.10), calls=%async_computation | async-start | bytes 524288 | tf_op jit(solution)/shard_map/all_to_all | solution.py:15
  7.4 4.3 %copy-start.19 = (bf16[8,128,128]{2,1,0:T(8,128)(2,1)S(1)}, bf16[8,128,128]{2,1,0:T(8,128)(2,1)}, u32[]{:S(2)}) copy-start(bf16[8,128,128]{2,1,0:T(8,128)(2,1)} %param.29) | copy-start | bytes 786436
  7.7 4.3 %copy-start.20 = (bf16[8,128,128]{2,1,0:T(8,128)(2,1)S(1)}, bf16[8,128,128]{2,1,0:T(8,128)(2,1)}, u32[]{:S(2)}) copy-start(bf16[8,128,128]{2,1,0:T(8,128)(2,1)} %param.28) | copy-start | bytes 786436
  7.7 4.5 %copy-start.16 = (f32[1024]{0:T(1024)S(1)}, f32[1024]{0:T(1024)}, u32[]{:S(2)}) copy-start(f32[1024]{0:T(1024)} %param.30) | copy-start | bytes 12292
  7.7 4.5 %copy-start.10 = (f32[64,1024]{1,0:T(8,128)S(1)}, f32[64,1024]{1,0:T(8,128)}, u32[]{:S(2)}) copy-start(f32[64,1024]{1,0:T(8,128)} %param.23) | copy-start | bytes 786436
  7.7 4.8 %copy-start.2 = (bf16[2048,1024]{1,0:T(8,128)(2,1)S(1)}, bf16[2048,1024]{1,0:T(8,128)(2,1)}, u32[]{:S(2)}) copy-start(bf16[2048,1024]{1,0:T(8,128)(2,1)} %param.26) | copy-start | bytes 12582916
  11.7 0.8 copy-start.11
  12.2 3.4 %copy-start.1 = (bf16[2048,1024]{1,0:T(8,128)(2,1)S(1)}, bf16[2048,1024]{1,0:T(8,128)(2,1)}, u32[]{:S(2)}) copy-start(bf16[2048,1024]{1,0:T(8,128)(2,1)} %param.31) | copy-start | bytes 12582916
  12.3 3.4 %copy-start.8 = (bf16[64,1024]{1,0:T(8,128)(2,1)S(1)}, bf16[64,1024]{1,0:T(8,128)(2,1)}, u32[]{:S(2)}) copy-start(bf16[64,1024]{1,0:T(8,128)(2,1)} %param.21) | copy-start | bytes 393220
  12.5 4.0 %copy-start.7 = (f32[64,1024]{1,0:T(8,128)}, f32[64,1024]{1,0:T(8,128)S(1)}, u32[]{:S(2)}) copy-start(f32[64,1024]{1,0:T(8,128)S(1)} %fusion.36) | copy-start | bytes 786436
  13.5 7.2 %copy-start.12 = (s32[64,6]{0,1:T(8,128)S(1)}, s32[64,6]{0,1:T(8,128)}, u32[]{:S(2)}) copy-start(s32[64,6]{0,1:T(8,128)} %param.33) | copy-start | bytes 4612
  15.6 9.4 %copy-start.13 = (f32[2048]{0:T(1024)S(1)}, f32[2048]{0:T(1024)}, u32[]{:S(2)}) copy-start(f32[2048]{0:T(1024)} %param.32) | copy-start | bytes 24580
  17.3 5.0 %all-to-all-start.1 = ((bf16[2,64,1024]{2,1,0:T(8,128)(2,1)}), bf16[2,64,1024]{2,1,0:T(8,128)(2,1)S(1)}, u32[]{:S(2)}, u32[]{:S(2)}) async-start(bf16[2,64,1024]{2,1,0:T(8,128)(2,1)} %broadcast_in_dim.11), calls=%async_computation.1 | async-start | bytes 524288 | tf_op jit(solution)/shard_map/all_to_all | solution.py:15
  25.2 0.7 copy-start.3
  104.7 4.4 %copy-start.17 = (bf16[1,2048,256]{2,1,0:T(8,128)(2,1)S(1)}, bf16[1,2048,256]{2,1,0:T(8,128)(2,1)}, u32[]{:S(2)}) copy-start(bf16[1,2048,256]{2,1,0:T(8,128)(2,1)} %param.35) | copy-start | bytes 3145732
  109.1 1.4 copy-start.18
  121.0 6.2 %copy-start.15 = (f32[64,6]{0,1:T(8,128)S(1)}, f32[64,6]{0,1:T(8,128)}, u32[]{:S(2)}) copy-start(f32[64,6]{0,1:T(8,128)} %param.34) | copy-start | bytes 4612
  121.0 6.9 %copy-start.4 = (bf16[64,2048]{1,0:T(8,128)(2,1)S(1)}, bf16[64,2048]{1,0:T(8,128)(2,1)}, u32[]{:S(2)}) copy-start(bf16[64,2048]{1,0:T(8,128)(2,1)} %copy-done.3) | copy-start | bytes 786436
  121.0 6.9 %copy-start.6 = (bf16[2048,256]{1,0:T(8,128)(2,1)S(1)}, bf16[2048,256]{1,0:T(8,128)(2,1)}, u32[]{:S(2)}) copy-start(bf16[2048,256]{1,0:T(8,128)(2,1)} %param.38) | copy-start | bytes 3145732
  121.0 48.4 %all-to-all-start.5 = ((bf16[64,18,1024]{2,1,0:T(8,128)(2,1)}), bf16[64,18,1024]{2,1,0:T(8,128)(2,1)}, u32[]{:S(2)}, u32[]{:S(2)}) async-start(bf16[64,18,1024]{2,1,0:T(8,128)(2,1)} %reshape.121), calls=%async_computation.5 | async-start | bytes 6291456 | tf_op jit(solution)/shard_map/all_to_all | solution.py:124
  127.0 4.8 %slice-start = ((bf16[64,3,1024]{2,0,1:T(8,128)(2,1)}), bf16[64,2,1024]{2,0,1:T(8,128)(2,1)S(1)}, s32[]{:S(2)}) async-start(bf16[64,3,1024]{2,0,1:T(8,128)(2,1)} %param.22), calls=%async_computation.6 | async-start | bytes 524288 | tf_op jit(solution)/shard_map/slice | solution.py:69
  127.0 4.8 %copy-start.9 = (bf16[64,1024]{1,0:T(8,128)(2,1)S(1)}, bf16[64,1024]{1,0:T(8,128)(2,1)}, u32[]{:S(2)}) copy-start(bf16[64,1024]{1,0:T(8,128)(2,1)} %get-tuple-element.18) | copy-start | bytes 393220
  175.1 2.8 %copy-start.14 = (f32[1024]{0:T(1024)S(1)}, f32[1024]{0:T(1024)}, u32[]{:S(2)}) copy-start(f32[1024]{0:T(1024)} %param.41) | copy-start | bytes 12292
